TPU v7x, 32 devices: a whole 2x2x4 slice. The times are simulated.
32 devices in a mesh: sp: 8 (over z, y), tp: 4 (over x, core).
Axes of the slice: x: 2, y: 2, z: 4, core: 2. Of those that a mesh axis runs over, the one named last changes fastest.
Arguments:
- tokens: bfloat16 [3072, 2048], P('sp', 'tp'), may hold values from -16 to 16
- norm_gain: bfloat16 [2048], replicated, may hold values from 0.099609375 to 1.8984375
- w_query: bfloat16 [2048, 1024], P(None, 'tp'), may hold values from -0.125 to 0.125
- w_key: bfloat16 [2048, 1024], P(None, 'tp'), may hold values from -0.125 to 0.125
- w_value: bfloat16 [2048, 1024], P(None, 'tp'), may hold values from -0.125 to 0.125
- key_bias: bfloat16 [8, 3072], P('tp', 'sp'), may hold values from -13 to 0
- w_glu_value: bfloat16 [2048, 1024], P(None, 'tp'), may hold values from -0.125 to 0.125
- w_glu_gate: bfloat16 [2048, 1024], P(None, 'tp'), may hold values from -0.125 to 0.125
- conv_weight: bfloat16 [31, 1024], replicated, may hold values from -4 to 4
- conv_bias: bfloat16 [1024], replicated, may hold values from 0 to 16
- ln_gain: bfloat16 [1024], replicated, may hold values from 0.099609375 to 1.8984375
- w_out_att: bfloat16 [1024, 2048], replicated, may hold values from -0.75 to 0.75
- w_out_conv: bfloat16 [1024, 2048], replicated, may hold values from -0.1875 to 0.1875
Outputs:
- mixed: bfloat16 [3072, 2048], P(('sp', 'tp'))
- weight_log: float32 [8, 3072], P('tp', 'sp')
All inputs are finite; a program needn't handle non-finite values.
Results may differ from a plain program's by a relative error of at most 0.007.
Values may be sent and summed in bfloat16 or wider, within the bound.
A program may use at most 192 MiB of HBM per device.

v0:
```python
import jax
import jax.numpy as jnp
from jax import lax
from jax.sharding import PartitionSpec as P

D = 2048
HEAD = 128
CF_WIDTH = 1024
epsilon = 1e-06


def from_behind(block, axis, distance):
    devices = range(lax.axis_size(axis))
    route = [(i - distance, i) for i in devices if i - distance in devices]
    return lax.ppermute(block, axis, route)


def rounded(values):
    return lax.optimization_barrier(values.astype(jnp.bfloat16)).astype(jnp.float32)


def later_matrix(count):
    row_ids = lax.broadcasted_iota(jnp.int32, (count, count), 0)
    col_ids = lax.broadcasted_iota(jnp.int32, (count, count), 1)
    return (row_ids > col_ids).astype(jnp.float32)


def block_terms(query_matrix_rows, key_rows, value_rows, bias_rows):
    head_size = query_matrix_rows.shape[-1]
    scores = jnp.einsum(
        "qhe,khe->hqk", query_matrix_rows, key_rows, preferred_element_type=jnp.float32
    )
    scores = scores * head_size ** (-0.5) + bias_rows.astype(jnp.float32)[:, None, :]
    keep_log = jax.nn.log_sigmoid(-scores)
    row_ids = lax.broadcasted_iota(jnp.int32, scores.shape, 1)
    col_ids = lax.broadcasted_iota(jnp.int32, scores.shape, 2)
    allowed = col_ids <= row_ids
    keep_log = jnp.where(allowed, keep_log, 0.0)
    later_sum = jnp.einsum(
        "hqj,jk->hqk", keep_log, later_matrix(scores.shape[2]), precision=lax.Precision.HIGHEST
    )
    weights = jnp.exp(jax.nn.log_sigmoid(scores) + later_sum)
    weights = jnp.where(allowed, weights, 0.0)
    block_out = jnp.einsum(
        "hqk,khe->qhe", weights.astype(jnp.bfloat16), value_rows, preferred_element_type=jnp.float32
    )
    return (block_out, jnp.sum(keep_log, axis=2))


def window_terms(query_matrix_rows, key_window, value_window, bias_window, valid_count):
    tok_rows, heads_here, head_size = query_matrix_rows.shape
    block_count = key_window.shape[0] // tok_rows
    key_blocks = key_window.reshape(block_count, tok_rows, heads_here, head_size)
    value_blocks = value_window.reshape(block_count, tok_rows, heads_here, head_size)
    bias_blocks = bias_window.astype(jnp.float32).reshape(heads_here, block_count, tok_rows)
    scores = jnp.einsum(
        "qhe,bkhe->hqbk", query_matrix_rows, key_blocks, preferred_element_type=jnp.float32
    )
    scores = scores * head_size ** (-0.5) + bias_blocks[:, None, :, :]
    block_ids = lax.broadcasted_iota(jnp.int32, scores.shape, 2)
    valid = block_ids < valid_count
    keep_log = jnp.where(valid, jax.nn.log_sigmoid(-scores), 0.0)
    later_sum = jnp.einsum(
        "hqbj,jk->hqbk", keep_log, later_matrix(tok_rows), precision=lax.Precision.HIGHEST
    )
    weights = jnp.where(valid, jnp.exp(jax.nn.log_sigmoid(scores) + later_sum), 0.0)
    block_out = jnp.einsum(
        "hqbk,bkhe->bqhe",
        weights.astype(jnp.bfloat16),
        value_blocks,
        preferred_element_type=jnp.float32,
    )
    totals = jnp.sum(keep_log, axis=3)
    after = jnp.einsum(
        "hqj,jb->hqb", totals, later_matrix(block_count), precision=lax.Precision.HIGHEST
    )
    factor = jnp.transpose(jnp.exp(after), (2, 1, 0))[:, :, :, None]
    return (jnp.sum(factor * block_out, axis=0), jnp.sum(totals, axis=2))


def combine(attended_sum, carried, block_out, block_keep):
    factor = jnp.exp(carried).T[:, :, None]
    return (attended_sum + factor * block_out, carried + block_keep)


def on_device(
    tokens,
    norm_gain,
    w_query,
    w_key,
    w_value,
    key_bias,
    w_glu_value,
    w_glu_gate,
    conv_weight,
    conv_bias,
    ln_gain,
    w_out_att,
    w_out_conv,
):
    tok_rows = tokens.shape[0]
    tp_count = lax.axis_size("tp")
    tp_index = lax.axis_index("tp")
    sp_index = lax.axis_index("sp")
    squares = jnp.sum(jnp.square(tokens.astype(jnp.float32)), axis=1)
    row_scale = lax.rsqrt(lax.psum(squares, "tp") / D + epsilon)
    matrices = (w_query, w_key, w_value, w_glu_value, w_glu_gate)
    gain_piece = norm_gain.astype(jnp.float32)
    normed = (
        lax.all_gather(tokens, "tp", axis=1, tiled=True).astype(jnp.float32)
        * row_scale[:, None]
        * gain_piece
    ).astype(jnp.bfloat16)
    projected = tuple(
        (jnp.dot(normed, matrix, preferred_element_type=jnp.float32) for matrix in matrices)
    )
    heads_here = w_query.shape[1] // HEAD
    query_matrix_rows = projected[0].astype(jnp.bfloat16).reshape(tok_rows, heads_here, HEAD)
    key_rows = projected[1].astype(jnp.bfloat16).reshape(tok_rows, heads_here, HEAD)
    value_rows = projected[2].astype(jnp.bfloat16).reshape(tok_rows, heads_here, HEAD)
    glu_value = rounded(projected[3])
    glu_gate = rounded(projected[4])
    attended_sum, carried = block_terms(query_matrix_rows, key_rows, value_rows, key_bias)
    every_key, every_value, every_bias = (
        lax.all_gather(key_rows, "sp", axis=0, tiled=True),
        lax.all_gather(value_rows, "sp", axis=0, tiled=True),
        lax.all_gather(key_bias, "sp", axis=1, tiled=True),
    )
    window_out, window_keep = window_terms(
        query_matrix_rows, every_key, every_value, every_bias, sp_index
    )
    attended_sum, carried = combine(attended_sum, carried, window_out, window_keep)
    attended = attended_sum.astype(jnp.bfloat16).reshape(tok_rows, heads_here * HEAD)
    weight_log = jnp.log(-jnp.expm1(carried))
    channels_here = w_glu_value.shape[1]
    channel_start = tp_index * channels_here
    taps_here = lax.dynamic_slice_in_dim(conv_weight, channel_start, channels_here, 1)
    bias_here = lax.dynamic_slice_in_dim(conv_bias, channel_start, channels_here, 0).astype(
        jnp.float32
    )
    gain_here = lax.dynamic_slice_in_dim(ln_gain, channel_start, channels_here, 0).astype(
        jnp.float32
    )
    gated = (glu_value * jax.nn.sigmoid(glu_gate)).astype(jnp.bfloat16)
    rim_width = conv_weight.shape[0] - 1
    rim_rows = from_behind(gated[tok_rows - rim_width :], "sp", 1)
    extended = jnp.concatenate([rim_rows, gated], axis=0)
    convolved = lax.conv_general_dilated(
        extended[None],
        taps_here[:, None, :],
        (1,),
        [(0, 0)],
        dimension_numbers=("NWC", "WIO", "NWC"),
        feature_group_count=channels_here,
        preferred_element_type=jnp.float32,
    )[0]
    convolved = convolved + bias_here[None, :]
    channel_mean = lax.psum(jnp.sum(convolved, axis=1), "tp") / CF_WIDTH
    centered = convolved - channel_mean[:, None]
    channel_var = lax.psum(jnp.sum(centered * centered, axis=1), "tp") / CF_WIDTH
    conv_out = jax.nn.silu(centered * lax.rsqrt(channel_var + epsilon)[:, None] * gain_here).astype(
        jnp.bfloat16
    )
    att_width = attended.shape[1]
    att_weight = lax.dynamic_slice_in_dim(w_out_att, tp_index * att_width, att_width, 0)
    conv_rows_weight = lax.dynamic_slice_in_dim(w_out_conv, channel_start, channels_here, 0)
    first = jnp.dot(attended, att_weight, preferred_element_type=jnp.float32)
    second = jnp.dot(
        lax.slice_in_dim(conv_out, 0, tok_rows // tp_count * lax.axis_size("tp"), axis=0),
        conv_rows_weight,
        preferred_element_type=jnp.float32,
    )
    mixed = lax.psum_scatter(first + second, "tp", scatter_dimension=0, tiled=True).astype(
        jnp.bfloat16
    )
    return (mixed, weight_log)


def solution(mesh):
    in_specs = (
        P("sp", "tp"),
        P(),
        P(None, "tp"),
        P(None, "tp"),
        P(None, "tp"),
        P("tp", "sp"),
        P(None, "tp"),
        P(None, "tp"),
        P(),
        P(),
        P(),
        P(),
        P(),
    )
    out_specs = (P(("sp", "tp"), None), P("tp", "sp"))
    return jax.shard_map(
        on_device, mesh=mesh, in_specs=in_specs, out_specs=out_specs, check_vma=False
    )
```

profile of v0, /device:TPU:0, one launch (start us, length us, event | category | flops | bytes accessed | tf_op | source)
XLA Modules:
  0.0 181.4 jit_solution(2660870203256576240)
XLA Ops:
  7.2 0.0 copy-start
  7.2 0.0 all-gather.4.cloned.1.call-start
  7.2 0.7 all-gather.4.cloned.1.call-update
  7.9 0.0 all-gather.6.cloned.1.call-start
  8.0 0.7 convert_element_type.66
  8.7 1.2 multiply_reduce_fusion
  9.8 8.4 %psum.21 = f32[384]{0:T(512)S(1)} all-reduce(f32[384]{0:T(512)S(1)} %multiply_reduce_fusion), channel_id=1, replica_groups=mesh['sp'=8,'tp'=4] {'tp'}, use_global_device_ids=true, to_apply=%region_1.0 | all-reduce | flops 384 | bytes 3072 | tf_op jit(solution)/shard_map/psum | solution.py:106
  18.2 13.8 %all-gather.4.cloned.1.call-done = bf16[384,2048]{1,0:T(8,128)(2,1)} async-done(((bf16[384,512]{1,0:T(8,128)(2,1)}), bf16[384,2048]{1,0:T(8,128)(2,1)}) %all-gather.4.cloned.1.call-update) | async-done | bytes 1572880 | tf_op jit(solution)/shard_map/all_gather | solution.py:110
  32.0 3.1 %convolution_convert_fusion.2 = bf16[384,256]{0,1:T(8,128)(2,1)} fusion(bf16[2048,256]{1,0:T(8,128)(2,1)S(1)} %copy-done, bf16[384,2048]{1,0:T(8,128)(2,1)} %all-gather.4.cloned.1.call-done, f32[2048]{0:T(1024)S(1)} %convert_element_type.66, f32[384]{0:T(512)S(1)} %add_rsqrt_fusion.1), kind=kOutput, calls=%fused_computation.35 | convolution fusion | flops 405897216 | bytes 2827776 | tf_op jit(solution)/shard_map/dot_general | solution.py:115
  35.0 0.0 all-gather.6.cloned.1.call-update
  35.0 0.0 all-gather.8.cloned.1.call-start
  35.1 26.3 %all_gather.14 = bf16[2,3072]{1,0:T(2,128)(2,1)S(1)} all-gather(bf16[2,384]{1,0:T(2,128)(2,1)S(1)} %copy-done.3), channel_id=1, replica_groups=mesh['sp'=8,'tp'=4] {'sp'}, dimensions={1}, use_global_device_ids=true | all-gather | bytes 13824 | tf_op jit(solution)/shard_map/all_gather | solution.py:127
  61.4 0.8 dynamic-slice_convert_fusion.1
  62.3 0.8 dynamic-slice_convert_fusion
  63.0 0.7 dynamic-slice_bitcast_fusion
  63.7 1.9 %convolution_convert_fusion.1 = bf16[384,256]{1,0:T(8,128)(2,1)S(1)} fusion(bf16[2048,256]{1,0:T(8,128)(2,1)} %param.19, bf16[384,2048]{1,0:T(8,128)(2,1)S(1)} %copy-done.4, f32[2048]{0:T(1024)S(1)} %convert_element_type.66, f32[384]{0:T(512)S(1)} %add_rsqrt_fusion.1), kind=kOutput, calls=%fused_computation.34 | convolution fusion | flops 405897216 | bytes 2827776 | tf_op jit(solution)/shard_map/dot_general | solution.py:115
  65.6 0.6 convolution_convert_fusion
  66.3 0.1 multiply_convert_fusion.2
  66.4 3.4 %collective-permute-start = (bf16[30,256]{1,0:T(8,128)(2,1)S(1)}, bf16[30,256]{1,0:T(8,128)(2,1)S(1)}, u32[]{:S(2)}, u32[]{:S(2)}) collective-permute-start(bf16[30,256]{1,0:T(8,128)(2,1)S(1)} %slice.6), channel_id=1, source_target_pairs={{0,4},{4,8},{8,12},{12,16},{16,20},{20,24},{24,28},{1,5},{5,9},{9,... | collective-permute-start | bytes 46088 | tf_op jit(solution)/shard_map/ppermute | solution.py:15
  69.8 0.9 convolution_convert_fusion.3
  70.7 0.4 fusion.39
  71.2 0.9 convolution_convert_fusion.4
  72.1 2.7 %fusion.15 = bf16[2,384,384]{1,2,0:T(8,128)(2,1)} fusion(f32[2,384,384]{1,2,0:T(8,128)S(1)} %get-tuple-element.7, u8[384,384]{0,1:T(8,128)(4,1)S(1)} %get-tuple-element.6), kind=kOutput, calls=%fused_computation.24 | convolution fusion | flops 1366179840 | bytes 1916928 | tf_op jit(solution)/shard_map/hqj,jk->hqk/dot_general | solution.py:39
  74.8 0.6 fusion.23
  75.3 0.8 copy.31
  76.2 0.0 all-gather.8.cloned.1.call-update
  76.2 0.0 reduce-scatter.2.cloned.1.call-start
  76.2 0.1 maximum_bitcast_fusion
  76.5 1.0 convolution_select_fusion
  77.4 0.1 copy.37
  77.6 0.1 fusion.38
  77.8 6.0 %psum.22 = f32[384]{0:T(512)S(1)} all-reduce(f32[384]{0:T(512)S(1)} %fusion.38), channel_id=1, replica_groups=mesh['sp'=8,'tp'=4] {'tp'}, use_global_device_ids=true, to_apply=%region_6.7 | all-reduce | flops 384 | bytes 3072 | tf_op jit(solution)/shard_map/psum | solution.py:158
  83.8 0.2 multiply_reduce_fusion.1
  84.0 5.9 %psum.23 = f32[384]{0:T(512)S(1)} all-reduce(f32[384]{0:T(512)S(1)} %multiply_reduce_fusion.1), channel_id=1, replica_groups=mesh['sp'=8,'tp'=4] {'tp'}, use_global_device_ids=true, to_apply=%region_8.9 | all-reduce | flops 384 | bytes 3072 | tf_op jit(solution)/shard_map/psum | solution.py:160
  90.0 0.0 all-gather.6.cloned.1.call-done
  90.0 1.9 %copy.28 = bf16[3072,2,128]{2,0,1:T(8,128)(2,1)S(1)} copy(bf16[3072,2,128]{0,2,1:T(8,128)(2,1)} %all-gather.6.cloned.1.call-done) | data formatting | bytes 3145728 | tf_op jit(solution)/shard_map/all_gather | solution.py:125
  91.9 3.4 %fusion.8 = (u8[2,384,384]{1,2,0:T(8,128)(4,1)S(1)}, f32[2,384,8,384]{1,3,2,0:T(8,128)S(1)}) fusion(f32[2,8,384]{2,1,0:T(8,128)S(1)} %bitcast.79, bf16[384,2,128,1]{0,2,3,1:T(8,128)(2,1)S(1)} %bitcast.78, bf16[8,384,2,128]{3,1,0,2:T(8,128)(2,1)S(1)} %bitcast.71), kind=kOutput, calls=%fused_computation.17 | convolution fusion | flops 620199936 | bytes 11526144 | tf_op jit(solution)/shard_map/qhe,bkhe->hqbk/dot_general | solution.py:56
  95.3 7.6 %fusion.58 = (f32[2,384]{1,0:T(2,128)S(1)}, f32[2,384,8]{1,2,0:T(8,128)S(1)}) fusion(f32[2,8,384]{2,1,0:T(8,128)S(1)} %bitcast.80, f32[2,384,8,384]{1,3,2,0:T(8,128)S(1)} %get-tuple-element.9, u8[2,384,384]{1,2,0:T(8,128)(4,1)S(1)} %get-tuple-element.8, pred[8]{0:T(512)(128)(4,1)S(1)} %iota_compare_fusion.4), kind=kLoop, calls=%fused_computation.94 | loop fusion | flops 35382528 | bytes 9784328 | tf_op jit(solution)/shard_map/reduce_sum | solution.py:78
  102.9 0.1 fusion.19
  103.1 0.6 negate_log_fusion
  103.7 23.3 %fusion.4 = bf16[2,384,8,384]{1,3,2,0:T(8,128)(2,1)} fusion(f32[2,384,8,384]{1,3,2,0:T(8,128)S(1)} %get-tuple-element.9, f32[2,8,384]{2,1,0:T(8,128)S(1)} %bitcast.81, pred[8]{0:T(512)(128)(4,1)S(1)} %iota_compare_fusion.4, u8[2,384,384]{1,2,0:T(8,128)(4,1)S(1)} %get-tuple-element.8), kind=kOutput, calls=%fused_computation.5 | convolution fusion | flops 10933125120 | bytes 14475272 | tf_op jit(solution)/shard_map/hqbj,jk->hqbk/dot_general | solution.py:63
  127.0 4.1 %fusion.7 = f32[384,2,128]{0,2,1:T(8,128)S(1)} fusion(bf16[2,384,8,384]{1,3,2,0:T(8,128)(2,1)} %fusion.4, bf16[8,384,2,128]{3,1,0,2:T(8,128)(2,1)} %bitcast.83, f32[8,384,2]{1,2,0:T(2,128)S(1)} %copy.30), kind=kOutput, calls=%fused_computation.14 | convolution fusion | flops 605454336 | bytes 6709248 | tf_op jit(solution)/shard_map/hqbk,bkhe->bqhe/dot_general | solution.py:67
  131.1 0.3 fusion.18
  131.4 1.8 %fusion.21 = f32[384,2048]{1,0:T(8,128)S(1)} fusion(bf16[384,256]{0,1:T(8,128)(2,1)S(1)} %bitcast.72, bf16[1024,2048]{1,0:T(8,128)(2,1)} %param.24, s32[]{:T(128)S(6)} %select_n.45), kind=kOutput, calls=%fused_computation.42 | convolution fusion | flops 402653184 | bytes 4390916 | tf_op jit(solution)/shard_map/dot_general | solution.py:167
  133.3 3.6 %convolution_add_fusion = f32[384,2048]{1,0:T(8,128)} fusion(f32[384,2048]{1,0:T(8,128)S(1)} %fusion.21, bf16[1024,2048]{1,0:T(8,128)(2,1)} %param.25, s32[]{:T(128)S(6)} %select_n.45, f32[1,416,256]{2,1,0:T(8,128)S(1)} %reshape.44, f32[256]{0:T(256)S(1)} %dynamic-slice_convert_fusion, f32[384]{0:T(512)S(1)} %add_rsqrt_fusion, ...), kind=kOutput, calls=%fused_computation.16 | convolution fusion | flops 404324352 | bytes 7739396 | tf_op jit(solution)/shard_map/dot_general | solution.py:168
  136.9 0.0 reduce-scatter.2.cloned.1.call-update
  136.9 36.1 %reduce-scatter.2.cloned.1.call-done = f32[96,2048]{1,0:T(8,128)} async-done(((f32[384,2048]{1,0:T(8,128)}), f32[96,2048]{1,0:T(8,128)}) %reduce-scatter.2.cloned.1.call-update) | async-done | bytes 786448 | tf_op jit(solution)/shard_map/reduce_scatter | solution.py:173
  173.0 1.9 %convert_element_type.83 = bf16[96,2048]{1,0:T(8,128)(2,1)} convert(f32[96,2048]{1,0:T(8,128)} %reduce-scatter.2.cloned.1.call-done) | non-fusion elementwise | flops 196608 | bytes 1179648 | tf_op jit(solution)/shard_map/convert_element_type | solution.py:173
  (32 shorter events, 0.3 us)
Async XLA Ops:
  7.2 24.8 %copy-start = (bf16[2048,256]{1,0:T(8,128)(2,1)S(1)}, bf16[2048,256]{1,0:T(8,128)(2,1)}, u32[]{:S(2)}) copy-start(bf16[2048,256]{1,0:T(8,128)(2,1)} %param.16) | copy-start | bytes 3145732
  7.2 27.9 %copy-start.3 = (bf16[2,384]{1,0:T(2,128)(2,1)S(1)}, bf16[2,384]{1,0:T(2,128)(2,1)}, u32[]{:S(2)}) copy-start(bf16[2,384]{1,0:T(2,128)(2,1)} %param.18) | copy-start | bytes 4612
  7.2 24.8 %all-gather.4.cloned.1.call-start = ((), (), s32[]{:S(2)}) async-start(), calls=%async_computation.1 | async-start | bytes 1966080 | tf_op jit(solution)/shard_map/all_gather | solution.py:110
  7.9 82.0 %all-gather.6.cloned.1.call-start = ((), (), s32[]{:S(2)}) async-start(), calls=%async_computation.2 | async-start | bytes 1769472 | tf_op jit(solution)/shard_map/all_gather | solution.py:125
  31.9 31.8 %copy-start.4 = (bf16[384,2048]{1,0:T(8,128)(2,1)S(1)}, bf16[384,2048]{1,0:T(8,128)(2,1)}, u32[]{:S(2)}) copy-start(bf16[384,2048]{1,0:T(8,128)(2,1)} %all-gather.4.cloned.1.call-done) | copy-start | bytes 4718596
  35.0 91.9 %all-gather.8.cloned.1.call-start = ((), (), s32[]{:S(2)}) async-start(), calls=%async_computation.3 | async-start | bytes 1769472 | tf_op jit(solution)/shard_map/all_gather | solution.py:126
  61.4 4.2 %copy-start.5 = (bf16[2048,256]{1,0:T(8,128)(2,1)S(1)}, bf16[2048,256]{1,0:T(8,128)(2,1)}, u32[]{:S(2)}) copy-start(bf16[2048,256]{1,0:T(8,128)(2,1)} %param.20) | copy-start | bytes 3145732
  65.6 4.2 %copy-start.6 = (bf16[2048,256]{1,0:T(8,128)(2,1)S(1)}, bf16[2048,256]{1,0:T(8,128)(2,1)}, u32[]{:S(2)}) copy-start(bf16[2048,256]{1,0:T(8,128)(2,1)} %param.15) | copy-start | bytes 3145732
  66.3 4.5 %copy-start.1 = (bf16[384,256]{0,1:T(8,128)(2,1)S(1)}, bf16[384,256]{0,1:T(8,128)(2,1)}, u32[]{:S(2)}) copy-start(bf16[384,256]{0,1:T(8,128)(2,1)} %convolution_convert_fusion.2) | copy-start | bytes 589828
  66.3 4.9 %copy-start.7 = (bf16[2048,256]{1,0:T(8,128)(2,1)S(1)}, bf16[2048,256]{1,0:T(8,128)(2,1)}, u32[]{:S(2)}) copy-start(bf16[2048,256]{1,0:T(8,128)(2,1)} %param.17) | copy-start | bytes 3145732
  66.4 9.8 %collective-permute-start = (bf16[30,256]{1,0:T(8,128)(2,1)S(1)}, bf16[30,256]{1,0:T(8,128)(2,1)S(1)}, u32[]{:S(2)}, u32[]{:S(2)}) collective-permute-start(bf16[30,256]{1,0:T(8,128)(2,1)S(1)} %slice.6), channel_id=1, source_target_pairs={{0,4},{4,8},{8,12},{12,16},{16,20},{20,24},{24,28},{1,5},{5,9},{9,... | collective-permute-start | bytes 46088 | tf_op jit(solution)/shard_map/ppermute | solution.py:15
  74.8 1.7 copy-start.8
  76.2 96.8 %reduce-scatter.2.cloned.1.call-start = ((), (), s32[]{:S(2)}) async-start(), calls=%async_computation.4 | async-start | bytes 3932160 | tf_op jit(solution)/shard_map/reduce_scatter | solution.py:173
  127.0 4.2 %copy-start.2 = (bf16[2,384,384]{1,2,0:T(8,128)(2,1)S(1)}, bf16[2,384,384]{1,2,0:T(8,128)(2,1)}, u32[]{:S(2)}) copy-start(bf16[2,384,384]{1,2,0:T(8,128)(2,1)} %fusion.15) | copy-start | bytes 1769476
Sparse Core Ops, SparseCore 0:
  9.6 22.3 all-gather.3
  35.2 44.7 all-gather.5
  82.2 42.4 all-gather.7
  137.0 35.9 reduce-scatter.1
where the time goes:
time: 182 us; the launch traced here: 181 us
  waiting for transfers between devices  50.6 us (28%)
  matrix products  48.1 us (26%)
  blocking collectives  46.5 us (26%)
  other arithmetic  14.7 us (8%)
  between operations  14.1 us (8%)
  local copies, waits for them, and re-layouts  3.85 us (2%)
  starting transfers between devices  3.56 us (2%)
    reduce_scatter x1, waiting for transfers between devices, on_device(): lax.psum_scatter(first + second, 'tp', scatter_dimension=0, tiled=True)  36.1 us
    all_gather x1, blocking collectives, on_device(): lax.all_gather(key_bias, 'sp', axis=1, tiled=True)  26.3 us
    dot_general x1, matrix products, window_terms(): jnp.einsum('hqbj,jk->hqbk', keep_log, later_matrix(tok_rows), precision=l...  23.3 us
    all_gather x1, waiting for transfers between devices, on_device(): lax.all_gather(tokens, 'tp', axis=1, tiled=True).astype(jnp.float32)  13.8 us
    psum x1, blocking collectives, on_device(): row_scale = lax.rsqrt(lax.psum(squares, 'tp') / D + epsilon)  8.37 us
    reduce_sum x1, other arithmetic, window_terms(): return (jnp.sum(factor * block_out, axis=0), jnp.sum(totals, axis=2))  7.62 us
    dot_general x5, matrix products, on_device(): jnp.dot(normed, matrix, preferred_element_type=jnp.float32)  7.31 us
    psum x1, blocking collectives, on_device(): channel_mean = lax.psum(jnp.sum(convolved, axis=1), 'tp') / CF_WIDTH  5.98 us
  transfers between devices with their start and end apart: 5, of which 2 were waited for; matrix products, arithmetic and copies ran while one was open for 29% of the time, Pallas kernels for 0%

commit v1 on v0

--- a/solution.py
+++ b/solution.py
@@ -121,10 +121,14 @@
     glu_value = rounded(projected[3])
     glu_gate = rounded(projected[4])
     attended_sum, carried = block_terms(query_matrix_rows, key_rows, value_rows, key_bias)
+
+    def compute_bars(z_in, axis_key):
+        return jnp.concatenate(lax.all_gather(z_in, axis_name=axis_key), 1)
+
     every_key, every_value, every_bias = (
         lax.all_gather(key_rows, "sp", axis=0, tiled=True),
         lax.all_gather(value_rows, "sp", axis=0, tiled=True),
-        lax.all_gather(key_bias, "sp", axis=1, tiled=True),
+        compute_bars(key_bias, "sp"),
     )
     window_out, window_keep = window_terms(
         query_matrix_rows, every_key, every_value, every_bias, sp_index

time: 182 us -> 191 us (1.049)
  waiting for transfers between devices: 50.6 us -> 59.4 us
    all_gather x1, waiting for transfers between devices: 0.01 us -> 14.7 us  [on_device(): lax.all_gather(key_rows, 'sp', axis=0, tiled=True)]
    all_gather x1, waiting for transfers between devices: 13.8 us -> 0.02 us  [on_device(): lax.all_gather(tokens, 'tp', axis=1, tiled=True).astype(jnp.float32)]
    all_gather x1, waiting for transfers between devices: 0.01 us -> 7.62 us  [on_device(): lax.all_gather(value_rows, 'sp', axis=0, tiled=True)]
  transfers between devices with their start and end apart: 5 -> 5, of which waited for: 2 -> 3; matrix products, arithmetic and copies ran while one was open for 29% -> 27% of each run, Pallas kernels for 0% -> 0%
where the time goes in v1:
time: 191 us
  waiting for transfers between devices  59.4 us (31%)
  matrix products  48.1 us (25%)
  blocking collectives  47 us (25%)
  other arithmetic  14.7 us (8%)
  between operations  14.1 us (7%)
  local copies, waits for them, and re-layouts  3.85 us (2%)
  starting transfers between devices  3.57 us (2%)
    reduce_scatter x1, waiting for transfers between devices, on_device(): lax.psum_scatter(first + second, 'tp', scatter_dimension=0, tiled=True)  36.4 us
    all_gather x1, blocking collectives, compute_bars(): return jnp.concatenate(lax.all_gather(z_in, axis_name=axis_key), 1)  26.5 us
    dot_general x1, matrix products, window_terms(): jnp.einsum('hqbj,jk->hqbk', keep_log, later_matrix(tok_rows), precision=l...  23.3 us
    all_gather x1, waiting for transfers between devices, on_device(): lax.all_gather(key_rows, 'sp', axis=0, tiled=True)  14.7 us
    psum x1, blocking collectives, on_device(): row_scale = lax.rsqrt(lax.psum(squares, 'tp') / D + epsilon)  8.37 us
    reduce_sum x1, other arithmetic, window_terms(): return (jnp.sum(factor * block_out, axis=0), jnp.sum(totals, axis=2))  7.62 us
    all_gather x1, waiting for transfers between devices, on_device(): lax.all_gather(value_rows, 'sp', axis=0, tiled=True)  7.62 us
    dot_general x5, matrix products, on_device(): jnp.dot(normed, matrix, preferred_element_type=jnp.float32)  7.33 us
  transfers between devices with their start and end apart: 5, of which 3 were waited for; matrix products, arithmetic and copies ran while one was open for 27% of the time, Pallas kernels for 0%

profile of v1, /device:TPU:0, one launch (start us, length us, event | category | flops | bytes accessed | tf_op | source)
XLA Modules:
  0.0 190.7 jit_solution(14957023183957187456)
XLA Ops:
  7.2 0.0 all-gather.6.cloned.1.call-start
  7.2 0.7 all-gather.6.cloned.1.call-update
  7.9 0.0 all-gather.8.cloned.1.call-start
  8.0 0.7 convert_element_type.73
  8.7 1.2 multiply_reduce_fusion
  9.8 8.4 %psum.21 = f32[384]{0:T(512)S(1)} all-reduce(f32[384]{0:T(512)S(1)} %multiply_reduce_fusion), channel_id=1, replica_groups=mesh['sp'=8,'tp'=4] {'tp'}, use_global_device_ids=true, to_apply=%region_1.0 | all-reduce | flops 384 | bytes 3072 | tf_op jit(solution)/shard_map/psum | solution.py:106
  18.2 26.5 %all-gather.1 = bf16[8,2,384]{2,1,0:T(2,128)(2,1)S(1)} all-gather(bf16[1,2,384]{2,1,0:T(2,128)(2,1)} %bitcast.77), channel_id=2, replica_groups=mesh['sp'=8,'tp'=4] {'sp'}, dimensions={0}, use_global_device_ids=true | all-gather | bytes 13824 | tf_op jit(solution)/shard_map/all_gather | solution.py:126
  44.7 0.0 all-gather.6.cloned.1.call-done
  44.8 3.1 %convolution_convert_fusion.2 = bf16[384,256]{0,1:T(8,128)(2,1)} fusion(bf16[2048,256]{1,0:T(8,128)(2,1)S(1)} %copy-done, bf16[384,2048]{1,0:T(8,128)(2,1)} %all-gather.6.cloned.1.call-done, f32[2048]{0:T(1024)S(1)} %convert_element_type.73, f32[384]{0:T(512)S(1)} %add_rsqrt_fusion.1), kind=kOutput, calls=%fused_computation.35 | convolution fusion | flops 405897216 | bytes 2827776 | tf_op jit(solution)/shard_map/dot_general | solution.py:115
  47.8 0.0 all-gather.8.cloned.1.call-update
  47.8 0.0 all-gather.10.cloned.1.call-start
  48.0 0.8 dynamic-slice_convert_fusion.1
  48.8 0.8 dynamic-slice_convert_fusion
  49.6 0.7 dynamic-slice_bitcast_fusion
  50.3 1.9 convolution_convert_fusion.1
  52.2 0.6 convolution_convert_fusion
  52.8 0.1 multiply_convert_fusion.2
  53.0 3.4 %collective-permute-start = (bf16[30,256]{1,0:T(8,128)(2,1)S(1)}, bf16[30,256]{1,0:T(8,128)(2,1)S(1)}, u32[]{:S(2)}, u32[]{:S(2)}) collective-permute-start(bf16[30,256]{1,0:T(8,128)(2,1)S(1)} %slice.6), channel_id=1, source_target_pairs={{0,4},{4,8},{8,12},{12,16},{16,20},{20,24},{24,28},{1,5},{5,9},{9,... | collective-permute-start | bytes 46088 | tf_op jit(solution)/shard_map/ppermute | solution.py:15
  56.4 0.9 convolution_convert_fusion.3
  57.3 0.4 fusion.39
  57.8 0.9 convolution_convert_fusion.4
  58.6 2.7 %fusion.15 = bf16[2,384,384]{1,2,0:T(8,128)(2,1)} fusion(f32[2,384,384]{1,2,0:T(8,128)S(1)} %get-tuple-element.7, u8[384,384]{0,1:T(8,128)(4,1)S(1)} %get-tuple-element.6), kind=kOutput, calls=%fused_computation.24 | convolution fusion | flops 1366179840 | bytes 1916928 | tf_op jit(solution)/shard_map/hqj,jk->hqk/dot_general | solution.py:39
  61.3 0.6 fusion.23
  61.9 0.8 copy.49
  62.7 0.0 all-gather.10.cloned.1.call-update
  62.7 0.0 reduce-scatter.2.cloned.1.call-start
  62.8 0.1 maximum_bitcast_fusion
  63.0 1.0 convolution_select_fusion
  64.0 0.1 copy.57
  64.2 0.1 fusion.38
  64.3 6.1 %psum.22 = f32[384]{0:T(512)S(1)} all-reduce(f32[384]{0:T(512)S(1)} %fusion.38), channel_id=1, replica_groups=mesh['sp'=8,'tp'=4] {'tp'}, use_global_device_ids=true, to_apply=%region_6.7 | all-reduce | flops 384 | bytes 3072 | tf_op jit(solution)/shard_map/psum | solution.py:162
  70.4 0.2 multiply_reduce_fusion.1
  70.6 6.1 %psum.23 = f32[384]{0:T(512)S(1)} all-reduce(f32[384]{0:T(512)S(1)} %multiply_reduce_fusion.1), channel_id=1, replica_groups=mesh['sp'=8,'tp'=4] {'tp'}, use_global_device_ids=true, to_apply=%region_8.9 | all-reduce | flops 384 | bytes 3072 | tf_op jit(solution)/shard_map/psum | solution.py:164
  76.7 14.7 %all-gather.8.cloned.1.call-done = bf16[3072,2,128]{0,2,1:T(8,128)(2,1)} async-done(((bf16[384,2,128]{0,2,1:T(8,128)(2,1)}), bf16[3072,2,128]{0,2,1:T(8,128)(2,1)}) %all-gather.8.cloned.1.call-update) | async-done | bytes 1572880 | tf_op jit(solution)/shard_map/all_gather | solution.py:129
  91.3 1.9 copy.45
  93.3 3.4 %fusion.8 = (u8[2,384,384]{1,2,0:T(8,128)(4,1)S(1)}, f32[2,384,8,384]{1,3,2,0:T(8,128)S(1)}) fusion(f32[2,8,384]{2,1,0:T(8,128)S(1)} %copy.47, bf16[384,2,128,1]{0,2,3,1:T(8,128)(2,1)S(1)} %bitcast.76, bf16[8,384,2,128]{3,1,0,2:T(8,128)(2,1)S(1)} %bitcast.69), kind=kOutput, calls=%fused_computation.17 | convolution fusion | flops 620199936 | bytes 11526144 | tf_op jit(solution)/shard_map/qhe,bkhe->hqbk/dot_general | solution.py:56
  96.7 7.6 %fusion.58 = (f32[2,384]{1,0:T(2,128)S(1)}, f32[2,384,8]{1,2,0:T(8,128)S(1)}) fusion(f32[2,8,384]{2,1,0:T(8,128)S(1)} %copy.47, f32[2,384,8,384]{1,3,2,0:T(8,128)S(1)} %get-tuple-element.9, u8[2,384,384]{1,2,0:T(8,128)(4,1)S(1)} %get-tuple-element.8, pred[8]{0:T(512)(128)(4,1)S(1)} %iota_compare_fusion.4), kind=kLoop, calls=%fused_computation.94 | loop fusion | flops 35382528 | bytes 9784328 | tf_op jit(solution)/shard_map/reduce_sum | solution.py:78
  104.3 0.1 fusion.19
  104.5 0.6 negate_log_fusion
  105.1 23.3 %fusion.4 = bf16[2,384,8,384]{1,3,2,0:T(8,128)(2,1)} fusion(f32[2,384,8,384]{1,3,2,0:T(8,128)S(1)} %get-tuple-element.9, f32[2,8,384]{2,1,0:T(8,128)S(1)} %copy.47, pred[8]{0:T(512)(128)(4,1)S(1)} %iota_compare_fusion.4, u8[2,384,384]{1,2,0:T(8,128)(4,1)S(1)} %get-tuple-element.8), kind=kOutput, calls=%fused_computation.5 | convolution fusion | flops 10933125120 | bytes 14475272 | tf_op jit(solution)/shard_map/hqbj,jk->hqbk/dot_general | solution.py:63
  128.3 7.6 %all-gather.10.cloned.1.call-done = bf16[3072,2,128]{2,0,1:T(8,128)(2,1)} async-done(((bf16[384,2,128]{2,0,1:T(8,128)(2,1)}), bf16[3072,2,128]{2,0,1:T(8,128)(2,1)}) %all-gather.10.cloned.1.call-update) | async-done | bytes 1572880 | tf_op jit(solution)/shard_map/all_gather | solution.py:130
  136.0 4.1 %fusion.7 = f32[384,2,128]{0,2,1:T(8,128)S(1)} fusion(bf16[2,384,8,384]{1,3,2,0:T(8,128)(2,1)} %fusion.4, bf16[8,384,2,128]{3,1,0,2:T(8,128)(2,1)} %bitcast.78, f32[8,384,2]{1,2,0:T(2,128)S(1)} %copy.48), kind=kOutput, calls=%fused_computation.14 | convolution fusion | flops 605454336 | bytes 6709248 | tf_op jit(solution)/shard_map/hqbk,bkhe->bqhe/dot_general | solution.py:67
  140.1 0.3 fusion.18
  140.4 1.8 fusion.21
  142.2 3.6 %convolution_add_fusion = f32[384,2048]{1,0:T(8,128)} fusion(f32[384,2048]{1,0:T(8,128)S(1)} %fusion.21, bf16[1024,2048]{1,0:T(8,128)(2,1)} %param.25, s32[]{:T(128)S(6)} %select_n.45, f32[1,416,256]{2,1,0:T(8,128)S(1)} %reshape.48, f32[256]{0:T(256)S(1)} %dynamic-slice_convert_fusion, f32[384]{0:T(512)S(1)} %add_rsqrt_fusion, ...), kind=kOutput, calls=%fused_computation.16 | convolution fusion | flops 404324352 | bytes 7739396 | tf_op jit(solution)/shard_map/dot_general | solution.py:172
  145.8 0.0 reduce-scatter.2.cloned.1.call-update
  145.9 36.4 %reduce-scatter.2.cloned.1.call-done = f32[96,2048]{1,0:T(8,128)} async-done(((f32[384,2048]{1,0:T(8,128)}), f32[96,2048]{1,0:T(8,128)}) %reduce-scatter.2.cloned.1.call-update) | async-done | bytes 786448 | tf_op jit(solution)/shard_map/reduce_scatter | solution.py:177
  182.3 1.9 %convert_element_type.92 = bf16[96,2048]{1,0:T(8,128)(2,1)} convert(f32[96,2048]{1,0:T(8,128)} %reduce-scatter.2.cloned.1.call-done) | non-fusion elementwise | flops 196608 | bytes 1179648 | tf_op jit(solution)/shard_map/convert_element_type | solution.py:177
  (33 shorter events, 0.3 us)
Async XLA Ops:
  7.2 37.6 %copy-start = (bf16[2048,256]{1,0:T(8,128)(2,1)S(1)}, bf16[2048,256]{1,0:T(8,128)(2,1)}, u32[]{:S(2)}) copy-start(bf16[2048,256]{1,0:T(8,128)(2,1)} %param.16) | copy-start | bytes 3145732
  7.2 40.7 %copy-start.3 = (bf16[2,384]{1,0:T(2,128)(2,1)S(1)}, bf16[2,384]{1,0:T(2,128)(2,1)}, u32[]{:S(2)}) copy-start(bf16[2,384]{1,0:T(2,128)(2,1)} %param.18) | copy-start | bytes 4612
  7.2 37.5 %all-gather.6.cloned.1.call-start = ((), (), s32[]{:S(2)}) async-start(), calls=%async_computation.1 | async-start | bytes 1966080 | tf_op jit(solution)/shard_map/all_gather | solution.py:110
  7.9 83.4 %all-gather.8.cloned.1.call-start = ((), (), s32[]{:S(2)}) async-start(), calls=%async_computation.2 | async-start | bytes 1769472 | tf_op jit(solution)/shard_map/all_gather | solution.py:129
  44.7 5.5 %copy-start.4 = (bf16[384,2048]{1,0:T(8,128)(2,1)S(1)}, bf16[384,2048]{1,0:T(8,128)(2,1)}, u32[]{:S(2)}) copy-start(bf16[384,2048]{1,0:T(8,128)(2,1)} %all-gather.6.cloned.1.call-done) | copy-start | bytes 4718596
  47.8 88.1 %all-gather.10.cloned.1.call-start = ((), (), s32[]{:S(2)}) async-start(), calls=%async_computation.3 | async-start | bytes 1769472 | tf_op jit(solution)/shard_map/all_gather | solution.py:130
  47.9 4.2 %copy-start.5 = (bf16[2048,256]{1,0:T(8,128)(2,1)S(1)}, bf16[2048,256]{1,0:T(8,128)(2,1)}, u32[]{:S(2)}) copy-start(bf16[2048,256]{1,0:T(8,128)(2,1)} %param.20) | copy-start | bytes 3145732
  52.2 4.2 %copy-start.6 = (bf16[2048,256]{1,0:T(8,128)(2,1)S(1)}, bf16[2048,256]{1,0:T(8,128)(2,1)}, u32[]{:S(2)}) copy-start(bf16[2048,256]{1,0:T(8,128)(2,1)} %param.15) | copy-start | bytes 3145732
  52.8 4.5 %copy-start.1 = (bf16[384,256]{0,1:T(8,128)(2,1)S(1)}, bf16[384,256]{0,1:T(8,128)(2,1)}, u32[]{:S(2)}) copy-start(bf16[384,256]{0,1:T(8,128)(2,1)} %convolution_convert_fusion.2) | copy-start | bytes 589828
  52.8 4.9 %copy-start.7 = (bf16[2048,256]{1,0:T(8,128)(2,1)S(1)}, bf16[2048,256]{1,0:T(8,128)(2,1)}, u32[]{:S(2)}) copy-start(bf16[2048,256]{1,0:T(8,128)(2,1)} %param.17) | copy-start | bytes 3145732
  53.0 9.8 %collective-permute-start = (bf16[30,256]{1,0:T(8,128)(2,1)S(1)}, bf16[30,256]{1,0:T(8,128)(2,1)S(1)}, u32[]{:S(2)}, u32[]{:S(2)}) collective-permute-start(bf16[30,256]{1,0:T(8,128)(2,1)S(1)} %slice.6), channel_id=1, source_target_pairs={{0,4},{4,8},{8,12},{12,16},{16,20},{20,24},{24,28},{1,5},{5,9},{9,... | collective-permute-start | bytes 46088 | tf_op jit(solution)/shard_map/ppermute | solution.py:15
  61.3 1.7 copy-start.8
  62.7 119.5 %reduce-scatter.2.cloned.1.call-start = ((), (), s32[]{:S(2)}) async-start(), calls=%async_computation.4 | async-start | bytes 3932160 | tf_op jit(solution)/shard_map/reduce_scatter | solution.py:177
  136.0 4.2 %copy-start.2 = (bf16[2,384,384]{1,2,0:T(8,128)(2,1)S(1)}, bf16[2,384,384]{1,2,0:T(8,128)(2,1)}, u32[]{:S(2)}) copy-start(bf16[2,384,384]{1,2,0:T(8,128)(2,1)} %fusion.15) | copy-start | bytes 1769476
Sparse Core Ops, SparseCore 0:
  9.6 22.3 all-gather.5
  48.0 43.3 all-gather.7
  93.5 42.3 all-gather.9
  146.0 36.2 reduce-scatter.1
